TPU v7x, 32 devices: a whole 2x2x4 slice. The times are simulated.
32 devices in a mesh: ep: 4 (over y, x), tp: 8 (over z, core).
Axes of the slice: x: 2, y: 2, z: 4, core: 2. Of those that a mesh axis runs over, the one named last changes fastest.
Arguments:
- queries: bfloat16 [4096, 1024], P('ep', 'tp'), may hold values from -6 to 6
- keys: bfloat16 [4096, 256], P('ep'), may hold values from -6 to 6, as said below
- values: bfloat16 [4096, 256], P('ep'), may hold values from -6 to 6
- slopes: float32 [16], P('tp'), may hold values from 0.002 to 0.08
- sinks: float32 [16], P('tp'), may hold values from 2 to 6
- out_weight: bfloat16 [1024, 2048], P('tp'), may hold values from -0.1875 to 0.1875
- mix_gain: float32 [2048], replicated, may hold values from 0.1 to 1.9
- moe_input: bfloat16 [4096, 2048], P(('ep', 'tp')), may hold values from -6 to 6
- in_gain: float32 [2048], replicated, may hold values from 0.1 to 1.9
- out_gain: float32 [2048], replicated, may hold values from 0.1 to 1.9
- group_router: bfloat16 [2048, 4], replicated, may hold values from -0.125 to 0.125
- expert_router: bfloat16 [2048, 4], replicated, may hold values from -0.125 to 0.125
- routes: int32 [4096, 2], P(('ep', 'tp')), may hold values from 0 to 3, all different within a row; in each aligned block of 128 rows (0 to 127, 128 to 255, ...) at most 96 rows name the same one
- gate_weight: bfloat16 [4, 2048, 1024], P('ep', None, 'tp'), may hold values from -0.125 to 0.125
- up_weight: bfloat16 [4, 2048, 1024], P('ep', None, 'tp'), may hold values from -0.125 to 0.125
- down_weight: bfloat16 [4, 2048, 1024], P('ep', None, 'tp'), may hold values from -0.1875 to 0.1875
Outputs:
- mixer_output: bfloat16 [4096, 2048], P(('ep', 'tp'))
- moe_output: bfloat16 [4096, 2048], P(('ep', 'tp'))
Inputs may be any that keep to these rules, and one draw needn't show every extreme that they name: `keys`: keys share one value range with the queries. `routes`: A token names 2 different experts. Among the rows of one device no expert is named more than 96 times, a bound that some block reaches in every draw.
All inputs are finite; a program needn't handle non-finite values.
Results may differ from a plain program's by a relative error of at most 0.018.
Values may be sent and summed in bfloat16 or wider, within the bound.
No kernel may reach another device: no remote copies, remote signals or barrier semaphores. Data moves between devices by JAX's collectives and lax.ppermute only.
A program may use at most 128 MiB of HBM per device.

v0:
```python
import math
import jax
import jax.numpy as jnp
from jax import lax
from jax.sharding import PartitionSpec as P

HEADS = 16
HD = 64
KV_HEADS = 4
WINDOW = 128
eps = 1e-06


def shifted(block, axis, distance):
    devices = range(lax.axis_size(axis))
    route = [(i - distance, i) for i in devices if i - distance in devices]
    return lax.ppermute(block, axis, route)


def scale_rows(matrix, gain):
    mean_square = jnp.mean(matrix * matrix, axis=-1, keepdims=True)
    return matrix * lax.rsqrt(mean_square + eps) * gain


def per_device(
    queries,
    keys,
    values,
    slopes,
    sinks,
    out_weight,
    mix_gain,
    moe_input,
    in_gain,
    out_gain,
    group_router,
    expert_router,
    routes,
    gate_weight,
    up_weight,
    down_weight,
):
    rows_group = queries.shape[0]
    local_heads = slopes.shape[0]
    per_kv = HEADS // KV_HEADS
    kv_index = lax.axis_index("tp") * local_heads // per_kv
    own_keys = lax.dynamic_slice_in_dim(keys, kv_index * HD, HD, 1)
    own_values = lax.dynamic_slice_in_dim(values, kv_index * HD, HD, 1)
    rim_keys, rim_values = shifted(
        (own_keys[rows_group - WINDOW :], own_values[rows_group - WINDOW :]), "ep", 1
    )
    blocks = rows_group // WINDOW
    key_blocks = own_keys.reshape(blocks, WINDOW, HD)
    value_blocks = own_values.reshape(blocks, WINDOW, HD)
    key_span = jnp.concatenate(
        [jnp.concatenate([rim_keys[None], key_blocks[:-1]], axis=0), key_blocks], axis=1
    )
    value_span = jnp.concatenate(
        [jnp.concatenate([rim_values[None], value_blocks[:-1]], axis=0), value_blocks], axis=1
    )
    query_blocks = queries.reshape(blocks, WINDOW, local_heads, HD)
    scores = jnp.einsum(
        "nqhd,nsd->nhqs", query_blocks, key_span, preferred_element_type=jnp.float32
    ) * (1.0 / math.sqrt(HD))
    query_index = jnp.arange(WINDOW, dtype=jnp.int32)[:, None]
    key_index = jnp.arange(2 * WINDOW, dtype=jnp.int32)[None, :]
    distance = query_index + WINDOW - key_index
    key_position = (
        lax.axis_index("ep") * rows_group
        + jnp.arange(blocks, dtype=jnp.int32)[:, None, None] * WINDOW
        + key_index[None]
        - WINDOW
    )
    valid = ((distance >= 0) & (distance < WINDOW))[None] & (key_position >= 0)
    scores = scores - slopes[None, :, None, None] * distance.astype(jnp.float32)[None, None]
    scores = jnp.where(valid[:, None], scores, -jnp.inf)
    sink = sinks[None, :, None, None]
    top = jnp.maximum(jnp.max(scores, axis=-1, keepdims=True), sink)
    weights = jnp.exp(scores - top)
    denom = jnp.sum(weights, axis=-1, keepdims=True) + jnp.exp(sink - top)
    probs = (weights / denom).astype(jnp.bfloat16)
    attention = jnp.einsum("nhqs,nsd->nqhd", probs, value_span, preferred_element_type=jnp.float32)
    attention = attention.astype(jnp.bfloat16).reshape(rows_group, local_heads * HD)
    own_rows = moe_input.shape[0]
    projected = lax.psum_scatter(
        jnp.dot(attention, out_weight, preferred_element_type=jnp.float32).astype(jnp.bfloat16),
        "tp",
        scatter_dimension=0,
        tiled=True,
    ).astype(jnp.float32)
    mixer_output = scale_rows(projected, mix_gain).astype(jnp.bfloat16)
    normed = scale_rows(moe_input.astype(jnp.float32), in_gain).astype(jnp.bfloat16)
    group_logits = jnp.dot(normed, group_router, preferred_element_type=jnp.float32)
    expert_logits = jnp.dot(normed, expert_router, preferred_element_type=jnp.float32)
    experts = expert_router.shape[1]
    groups = group_router.shape[1]
    per_group = experts // groups
    visits = routes.shape[1]
    expert_match = routes[:, :, None] == jnp.arange(experts, dtype=jnp.int32)[None, None, :]
    picked_logits = jnp.sum(jnp.where(expert_match, expert_logits[:, None, :], 0.0), axis=-1)
    group_prob = jax.nn.softmax(group_logits, axis=-1)
    group_match = (routes // per_group)[:, :, None] == jnp.arange(groups, dtype=jnp.int32)[
        None, None, :
    ]
    picked_group = jnp.sum(jnp.where(group_match, group_prob[:, None, :], 0.0), axis=-1)
    route_weight = picked_group * jax.nn.softmax(picked_logits, axis=-1)
    capacity = max(2, 3 * own_rows * visits // (2 * experts))
    match_int = expert_match.astype(jnp.int32).reshape(own_rows * visits, experts)
    before = jnp.cumsum(match_int, axis=0) - match_int
    slot = jnp.sum(before * match_int, axis=-1)
    position = (routes.reshape(-1) * capacity + slot).reshape(own_rows, visits)
    slot_ids = jnp.arange(experts * capacity, dtype=jnp.int32)
    placement = jnp.any(position[None, :, :] == slot_ids[:, None, None], axis=-1).astype(
        jnp.bfloat16
    )
    outgoing = jnp.dot(placement, normed, preferred_element_type=jnp.float32).astype(jnp.bfloat16)
    local_experts = gate_weight.shape[0]
    outgoing = outgoing.reshape(lax.axis_size("ep"), local_experts, capacity, normed.shape[1])
    arrived = lax.all_to_all(outgoing, "ep", split_axis=0, concat_axis=0, tiled=True)
    gate_piece = lax.all_gather(gate_weight, "tp", axis=2, tiled=True)
    up_piece = lax.all_gather(up_weight, "tp", axis=2, tiled=True)
    down_piece = lax.all_gather(down_weight, "tp", axis=2, tiled=True)
    gate = jnp.einsum("sxcd,xdf->sxcf", arrived, gate_piece, preferred_element_type=jnp.float32)
    up = jnp.einsum("sxcd,xdf->sxcf", arrived, up_piece, preferred_element_type=jnp.float32)
    hidden = (jax.nn.silu(gate) * up).astype(jnp.bfloat16)
    results = jnp.einsum("sxcf,xdf->sxcd", hidden, down_piece, preferred_element_type=jnp.float32)
    returned = lax.all_to_all(
        results.astype(jnp.bfloat16), "ep", split_axis=0, concat_axis=0, tiled=True
    )
    flat_back = returned.reshape(experts * capacity, returned.shape[3])
    picked_rows = jnp.take(flat_back, position.reshape(-1), axis=0).reshape(
        own_rows, visits, flat_back.shape[1]
    )
    moe = jnp.sum(route_weight[:, :, None] * picked_rows.astype(jnp.float32), axis=1)
    moe_output = scale_rows(moe, out_gain).astype(jnp.bfloat16)
    return (mixer_output, moe_output)


def solution(mesh):
    return jax.shard_map(
        per_device,
        mesh=mesh,
        in_specs=(
            P("ep", "tp"),
            P("ep", None),
            P("ep", None),
            P("tp"),
            P("tp"),
            P("tp", None),
            P(),
            P(("ep", "tp"), None),
            P(),
            P(),
            P(),
            P(),
            P(("ep", "tp"), None),
            P("ep", None, "tp"),
            P("ep", None, "tp"),
            P("ep", None, "tp"),
        ),
        out_specs=(P(("ep", "tp"), None), P(("ep", "tp"), None)),
        check_vma=False,
    )
```

profile of v0, /device:TPU:0, one launch (start us, length us, event | category | flops | bytes accessed | tf_op | source)
XLA Modules:
  0.0 222.8 jit_solution(3067624268574023449)
XLA Ops:
  7.2 0.7 all-gather.6.cloned.1.call-update
  8.0 0.7 all-gather.4.cloned.1.call-update
  8.7 0.7 all-gather.8.cloned.1.call-update
  9.5 1.2 constant_dynamic-slice_fusion
  10.9 4.9 %collective-permute-start.1 = (bf16[128,64]{0,1:T(8,128)(2,1)S(1)}, bf16[128,64]{0,1:T(8,128)(2,1)S(1)}, u32[]{:S(2)}, u32[]{:S(2)}) collective-permute-start(bf16[128,64]{0,1:T(8,128)(2,1)S(1)} %slice.36), channel_id=1, source_target_pairs={{0,8},{8,16},{16,24},{1,9},{9,17},{17,25},{2,10},{10,18},{18,26},{... | collective-permute-start | bytes 49160 | tf_op jit(solution)/shard_map/ppermute | solution.py:17
  15.9 3.4 %collective-permute-start = (bf16[128,64]{0,1:T(8,128)(2,1)S(1)}, bf16[128,64]{0,1:T(8,128)(2,1)S(1)}, u32[]{:S(2)}, u32[]{:S(2)}) collective-permute-start(bf16[128,64]{0,1:T(8,128)(2,1)S(1)} %slice.34), channel_id=1, source_target_pairs={{0,8},{8,16},{16,24},{1,9},{9,17},{17,25},{2,10},{10,18},{18,26},{... | collective-permute-start | bytes 49160 | tf_op jit(solution)/shard_map/ppermute | solution.py:17
  19.6 0.3 broadcast_and_fusion
  20.1 0.2 reshape.313
  20.3 0.6 fusion.73
  21.1 0.3 fusion.13
  21.5 0.5 fusion.20
  22.2 3.2 %convolution_convert_fusion = bf16[1024,2048]{1,0:T(8,128)(2,1)} fusion(bf16[128,2048]{1,0:T(8,128)(2,1)S(1)} %copy-done, bf16[16,8,8,128]{3,2,1,0:T(8,128)(2,1)S(1)} %bitcast.155), kind=kOutput, calls=%fused_computation.7 | convolution fusion | flops 538968064 | bytes 4980736 | tf_op jit(solution)/shard_map/dot_general | solution.py:86
  25.4 0.6 copy-done.3
  26.5 1.2 reduce-window.6
  28.6 1.8 convolution_convert_fusion.1
  30.4 3.9 %all-to-all-start = ((bf16[4,1,96,2048]{3,2,1,0:T(8,128)(2,1)}), bf16[4,1,96,2048]{3,2,1,0:T(8,128)(2,1)S(1)}, u32[]{:S(2)}, u32[]{:S(2)}) async-start(bf16[4,1,96,2048]{3,2,1,0:T(8,128)(2,1)} %bitcast.11), calls=%async_computation.1 | async-start | bytes 3145728 | tf_op jit(solution)/shard_map/all_to_all | solution.py:119
  34.3 0.3 fusion.74
  34.7 0.3 fusion.68
  35.5 17.6 %all-to-all-done = bf16[4,1,96,2048]{3,2,1,0:T(8,128)(2,1)S(1)} async-done(((bf16[4,1,96,2048]{3,2,1,0:T(8,128)(2,1)}), bf16[4,1,96,2048]{3,2,1,0:T(8,128)(2,1)S(1)}, u32[]{:S(2)}, u32[]{:S(2)}) %all-to-all-start) | async-done | bytes 1572896 | tf_op jit(solution)/shard_map/all_to_all | solution.py:119
  53.1 7.1 %all-gather.6.cloned.1.call-done = bf16[1,2048,1024]{2,1,0:T(8,128)(2,1)} async-done(((bf16[1,2048,128]{2,1,0:T(8,128)(2,1)}), bf16[1,2048,1024]{2,1,0:T(8,128)(2,1)}) %all-gather.6.cloned.1.call-update) | async-done | bytes 4194320 | tf_op jit(solution)/shard_map/all_gather | solution.py:121
  60.2 5.1 %fusion.2 = f32[4,96,1024]{2,1,0:T(8,128)} fusion(bf16[1,2048,1024]{2,1,0:T(8,128)(2,1)} %all-gather.6.cloned.1.call-done, bf16[4,1,96,2048]{3,2,1,0:T(8,128)(2,1)S(1)} %all-to-all-done), kind=kOutput, calls=%fused_computation.3 | convolution fusion | flops 1610612736 | bytes 7340032 | tf_op jit(solution)/shard_map/sxcd,xdf->sxcf/dot_general | solution.py:124
  65.3 42.5 %all-gather.4.cloned.1.call-done = bf16[1,2048,1024]{2,1,0:T(8,128)(2,1)} async-done(((bf16[1,2048,128]{2,1,0:T(8,128)(2,1)}), bf16[1,2048,1024]{2,1,0:T(8,128)(2,1)}) %all-gather.4.cloned.1.call-update) | async-done | bytes 4194320 | tf_op jit(solution)/shard_map/all_gather | solution.py:120
  107.8 47.6 %all-gather.8.cloned.1.call-done = bf16[1,2048,1024]{2,1,0:T(8,128)(2,1)} async-done(((bf16[1,2048,128]{2,1,0:T(8,128)(2,1)}), bf16[1,2048,1024]{2,1,0:T(8,128)(2,1)}) %all-gather.8.cloned.1.call-update) | async-done | bytes 4194320 | tf_op jit(solution)/shard_map/all_gather | solution.py:122
  155.4 8.6 %fusion.9 = bf16[4,1,96,2048]{3,2,1,0:T(8,128)(2,1)} fusion(bf16[1,2048,1024]{2,1,0:T(8,128)(2,1)} %all-gather.8.cloned.1.call-done, f32[4,96,1024]{2,1,0:T(8,128)} %fusion.2, bf16[1,2048,1024]{2,1,0:T(8,128)(2,1)} %all-gather.4.cloned.1.call-done, bf16[4,1,96,2048]{3,2,1,0:T(8,128)(2,1)S(1)} %all-to-all-done), kind=kOutput, calls=%fused_computation.10 | convolution fusion | flops 3224371200 | bytes 13107200 | tf_op jit(solution)/shard_map/sxcf,xdf->sxcd/dot_general | solution.py:126
  164.1 3.9 %all-to-all-start.1 = ((bf16[4,1,96,2048]{3,2,1,0:T(8,128)(2,1)}), bf16[4,1,96,2048]{3,2,1,0:T(8,128)(2,1)S(1)}, u32[]{:S(2)}, u32[]{:S(2)}) async-start(bf16[4,1,96,2048]{3,2,1,0:T(8,128)(2,1)} %fusion.9), calls=%async_computation.2 | async-start | bytes 3145728 | tf_op jit(solution)/shard_map/all_to_all | solution.py:127
  168.1 37.6 %reduce-scatter.2.cloned.1.call-done = bf16[128,2048]{1,0:T(8,128)(2,1)} async-done(((bf16[1024,2048]{1,0:T(8,128)(2,1)}), bf16[128,2048]{1,0:T(8,128)(2,1)}) %reduce-scatter.2.cloned.1.call-update) | async-done | bytes 524304 | tf_op jit(solution)/shard_map/reduce_scatter | solution.py:85
  205.7 1.2 fusion.30
  207.0 2.0 fusion.32
  209.0 1.4 gather_fusion
  210.4 0.7 gather.7
  211.1 4.1 %multiply_reduce_fusion = f32[128,2048]{1,0:T(8,128)S(1)} fusion(bf16[128,2,2048]{2,1,0:T(2,128)(2,1)S(1)} %gather.7, pred[128,2]{1,0:T(8,128)(4,1)S(1)} %copy.102, f32[128,2]{1,0:T(8,128)S(1)} %copy.96), kind=kLoop, calls=%fused_computation.13 | loop fusion | flops 1835008 | bytes 2098432 | tf_op jit(solution)/shard_map/reduce_sum | solution.py:134
  215.3 1.0 multiply_convert_fusion
  (79 shorter events, 3.2 us)
Async XLA Ops:
  7.2 15.0 %copy-start = (bf16[128,2048]{1,0:T(8,128)(2,1)S(1)}, bf16[128,2048]{1,0:T(8,128)(2,1)}, u32[]{:S(2)}) copy-start(bf16[128,2048]{1,0:T(8,128)(2,1)} %param.21) | copy-start | bytes 1572868
  7.2 53.0 %all-gather.6.cloned.1.call-start = ((), (), s32[]{:S(2)}) async-start(), calls=%async_computation.5 | async-start | bytes 4718592 | tf_op jit(solution)/shard_map/all_gather | solution.py:121
  7.9 12.0 %copy-start.8 = (f32[2]{0:T(128)S(1)}, f32[2]{0:T(128)}, u32[]{:S(2)}) copy-start(f32[2]{0:T(128)} %param.19) | copy-start | bytes 28
  7.9 99.9 %all-gather.4.cloned.1.call-start = ((), (), s32[]{:S(2)}) async-start(), calls=%async_computation.4 | async-start | bytes 4718592 | tf_op jit(solution)/shard_map/all_gather | solution.py:120
  8.7 11.4 %copy-start.2 = (bf16[1024,128]{1,0:T(8,128)(2,1)S(1)}, bf16[1024,128]{1,0:T(8,128)(2,1)}, u32[]{:S(2)}) copy-start(bf16[1024,128]{1,0:T(8,128)(2,1)} %param.16) | copy-start | bytes 786436
  8.7 146.7 %all-gather.8.cloned.1.call-start = ((), (), s32[]{:S(2)}) async-start(), calls=%async_computation.6 | async-start | bytes 4718592 | tf_op jit(solution)/shard_map/all_gather | solution.py:122
  9.4 196.3 %reduce-scatter.2.cloned.1.call-start = ((), (), s32[]{:S(2)}) async-start(), calls=%async_computation.3 | async-start | bytes 4718592 | tf_op jit(solution)/shard_map/reduce_scatter | solution.py:85
  10.9 9.4 %collective-permute-start.1 = (bf16[128,64]{0,1:T(8,128)(2,1)S(1)}, bf16[128,64]{0,1:T(8,128)(2,1)S(1)}, u32[]{:S(2)}, u32[]{:S(2)}) collective-permute-start(bf16[128,64]{0,1:T(8,128)(2,1)S(1)} %slice.36), channel_id=1, source_target_pairs={{0,8},{8,16},{16,24},{1,9},{9,17},{17,25},{2,10},{10,18},{18,26},{... | collective-permute-start | bytes 49160 | tf_op jit(solution)/shard_map/ppermute | solution.py:17
  15.9 5.6 %collective-permute-start = (bf16[128,64]{0,1:T(8,128)(2,1)S(1)}, bf16[128,64]{0,1:T(8,128)(2,1)S(1)}, u32[]{:S(2)}, u32[]{:S(2)}) collective-permute-start(bf16[128,64]{0,1:T(8,128)(2,1)S(1)} %slice.34), channel_id=1, source_target_pairs={{0,8},{8,16},{16,24},{1,9},{9,17},{17,25},{2,10},{10,18},{18,26},{... | collective-permute-start | bytes 49160 | tf_op jit(solution)/shard_map/ppermute | solution.py:17
  20.3 0.7 copy-start.7
  25.4 0.7 copy-start.3
  25.4 3.0 %copy-start.1 = (bf16[128,2048]{1,0:T(8,128)(2,1)S(1)}, bf16[128,2048]{1,0:T(8,128)(2,1)}, u32[]{:S(2)}) copy-start(bf16[128,2048]{1,0:T(8,128)(2,1)} %param.23) | copy-start | bytes 1572868
  25.4 3.2 %copy-start.4 = (f32[2048]{0:T(1024)S(1)}, f32[2048]{0:T(1024)}, u32[]{:S(2)}) copy-start(f32[2048]{0:T(1024)} %param.24) | copy-start | bytes 24580
  30.4 3.9 %copy-start.9 = (bf16[2048,4]{0,1:T(4,128)(2,1)S(1)}, bf16[2048,4]{0,1:T(4,128)(2,1)}, u32[]{:S(2)}) copy-start(bf16[2048,4]{0,1:T(4,128)(2,1)} %param.26) | copy-start | bytes 49156
  30.4 4.3 %copy-start.10 = (bf16[2048,4]{0,1:T(4,128)(2,1)S(1)}, bf16[2048,4]{0,1:T(4,128)(2,1)}, u32[]{:S(2)}) copy-start(bf16[2048,4]{0,1:T(4,128)(2,1)} %param.27) | copy-start | bytes 49156
  30.4 22.6 %all-to-all-start = ((bf16[4,1,96,2048]{3,2,1,0:T(8,128)(2,1)}), bf16[4,1,96,2048]{3,2,1,0:T(8,128)(2,1)S(1)}, u32[]{:S(2)}, u32[]{:S(2)}) async-start(bf16[4,1,96,2048]{3,2,1,0:T(8,128)(2,1)} %bitcast.11), calls=%async_computation.1 | async-start | bytes 3145728 | tf_op jit(solution)/shard_map/all_to_all | solution.py:119
  164.1 42.9 %copy-start.5 = (f32[2048]{0:T(1024)S(1)}, f32[2048]{0:T(1024)}, u32[]{:S(2)}) copy-start(f32[2048]{0:T(1024)} %param.22) | copy-start | bytes 24580
  164.1 44.9 %all-to-all-start.1 = ((bf16[4,1,96,2048]{3,2,1,0:T(8,128)(2,1)}), bf16[4,1,96,2048]{3,2,1,0:T(8,128)(2,1)S(1)}, u32[]{:S(2)}, u32[]{:S(2)}) async-start(bf16[4,1,96,2048]{3,2,1,0:T(8,128)(2,1)} %fusion.9), calls=%async_computation.2 | async-start | bytes 3145728 | tf_op jit(solution)/shard_map/all_to_all | solution.py:127
  211.1 4.3 %copy-start.6 = (f32[2048]{0:T(1024)S(1)}, f32[2048]{0:T(1024)}, u32[]{:S(2)}) copy-start(f32[2048]{0:T(1024)} %param.25) | copy-start | bytes 24580
Sparse Core Ops, SparseCore 0:
  9.6 50.5 all-gather.5
  61.7 45.9 all-gather.3
  109.4 45.9 all-gather.7
  157.6 48.1 reduce-scatter.1
where the time goes:
time: 223 us
  waiting for transfers between devices  155 us (70%)
  matrix products  20.5 us (9%)
  starting transfers between devices  16.2 us (7%)
  between operations  14.2 us (6%)
  other arithmetic  11.3 us (5%)
  local copies, waits for them, and re-layouts  6.18 us (3%)
    all_gather x1, waiting for transfers between devices, per_device(): down_piece = lax.all_gather(down_weight, 'tp', axis=2, tiled=True)  47.6 us
    all_gather x1, waiting for transfers between devices, per_device(): gate_piece = lax.all_gather(gate_weight, 'tp', axis=2, tiled=True)  42.5 us
    reduce_scatter x1, waiting for transfers between devices, per_device(): lax.psum_scatter(jnp.dot(attention, out_weight, preferred_element_type=jn...  37.6 us
    all_to_all x1, waiting for transfers between devices, per_device(): lax.all_to_all(outgoing, 'ep', split_axis=0, concat_axis=0, tiled=True)  17.6 us
    dot_general x1, matrix products, per_device(): jnp.einsum('sxcf,xdf->sxcd', hidden, down_piece, preferred_element_type=j...  8.63 us
    ppermute x2, starting transfers between devices, shifted(): return lax.ppermute(block, axis, route)  8.27 us
    all_gather x1, waiting for transfers between devices, per_device(): up_piece = lax.all_gather(up_weight, 'tp', axis=2, tiled=True)  7.09 us
    dot_general x1, matrix products, per_device(): jnp.einsum('sxcd,xdf->sxcf', arrived, up_piece, preferred_element_type=jn...  5.13 us
  transfers between devices with their start and end apart: 8, of which 5 were waited for; matrix products, arithmetic and copies ran while one was open for 13% of the time, Pallas kernels for 0%

commit v1 on v0

--- a/solution.py
+++ b/solution.py
@@ -117,10 +117,25 @@
     local_experts = gate_weight.shape[0]
     outgoing = outgoing.reshape(lax.axis_size("ep"), local_experts, capacity, normed.shape[1])
     arrived = lax.all_to_all(outgoing, "ep", split_axis=0, concat_axis=0, tiled=True)
-    gate_piece = lax.all_gather(gate_weight, "tp", axis=2, tiled=True)
     up_piece = lax.all_gather(up_weight, "tp", axis=2, tiled=True)
     down_piece = lax.all_gather(down_weight, "tp", axis=2, tiled=True)
-    gate = jnp.einsum("sxcd,xdf->sxcf", arrived, gate_piece, preferred_element_type=jnp.float32)
+    ways, here, step = (lax.axis_size("tp"), lax.axis_index("tp"), gate_weight.shape[2])
+    earlier, later = ([], [])
+    going_up = going_down = gate_weight
+    for far in range(ways // 2 + 1):
+        earlier.append(
+            jnp.einsum("sxcd,xdf->sxcf", arrived, going_up, preferred_element_type=jnp.float32)
+        )
+        if 0 < far < ways - ways // 2:
+            later.append(
+                jnp.einsum(
+                    "sxcd,xdf->sxcf", arrived, going_down, preferred_element_type=jnp.float32
+                )
+            )
+        going_up = lax.ppermute(going_up, "tp", [(d, (d + 1) % ways) for d in range(ways)])
+        going_down = lax.ppermute(going_down, "tp", [(d, (d - 1) % ways) for d in range(ways)])
+    line = jnp.concatenate([*earlier[::-1], *later], axis=3)
+    gate = jnp.roll(line, (here - ways // 2) * earlier[0].shape[3], axis=3)
     up = jnp.einsum("sxcd,xdf->sxcf", arrived, up_piece, preferred_element_type=jnp.float32)
     hidden = (jax.nn.silu(gate) * up).astype(jnp.bfloat16)
     results = jnp.einsum("sxcf,xdf->sxcd", hidden, down_piece, preferred_element_type=jnp.float32)

time: 223 us -> 208 us (0.933)
  waiting for transfers between devices: 155 us -> 109 us
  starting transfers between devices: 16.2 us -> 28.4 us
  matrix products: 20.5 us -> 31.8 us
  local copies, waits for them, and re-layouts: 6.18 us -> 12.2 us
    ppermute x0 -> x7, waiting for transfers between devices: none -> 71.4 us  [the longest x4 69.1 us: per_device(): lax.ppermute(going_up, 'tp', [(d, (d + 1) % ways) for d in range(ways)])]
    all_gather x1, waiting for transfers between devices: 47.6 us -> 0.01 us  [per_device(): down_piece = lax.all_gather(down_weight, 'tp', axis=2, tiled=True)]
    all_gather x1 -> x0, waiting for transfers between devices: 42.5 us -> none  [per_device(): gate_piece = lax.all_gather(gate_weight, 'tp', axis=2, tiled=True)]
    all_to_all x1, waiting for transfers between devices: 17.6 us -> 0.01 us  [per_device(): lax.all_to_all(outgoing, 'ep', split_axis=0, concat_axis=0, tiled=True)]
    dot_general x1 -> x8, matrix products: 5.13 us -> 16.5 us  [the longest x5 10.5 us: per_device(): jnp.einsum('sxcd,xdf->sxcf', arrived, going_up, preferred_element_type=jn...]
    ppermute x0 -> x7, starting transfers between devices: none -> 10.8 us  [the longest x3 10.8 us: per_device(): lax.ppermute(going_down, 'tp', [(d, (d - 1) % ways) for d in range(ways)])]
    all_gather x1, waiting for transfers between devices: 7.09 us -> 0.01 us  [per_device(): up_piece = lax.all_gather(up_weight, 'tp', axis=2, tiled=True)]
    unnamed x25 -> x34, local copies, waits for them, and re-layouts: 1.09 us -> 6.41 us
  transfers between devices with their start and end apart: 8 -> 14, of which waited for: 5 -> 6; matrix products, arithmetic and copies ran while one was open for 13% -> 23% of each run, Pallas kernels for 0% -> 0%
where the time goes in v1:
time: 208 us; the launch traced here: 207 us
  waiting for transfers between devices  109 us (52%)
  matrix products  31.8 us (15%)
  starting transfers between devices  28.4 us (14%)
  between operations  14.1 us (7%)
  local copies, waits for them, and re-layouts  12.2 us (6%)
  other arithmetic  11.3 us (5%)
    ppermute x4, waiting for transfers between devices, per_device(): lax.ppermute(going_up, 'tp', [(d, (d + 1) % ways) for d in range(ways)])  69.1 us
    reduce_scatter x1, waiting for transfers between devices, per_device(): lax.psum_scatter(jnp.dot(attention, out_weight, preferred_element_type=jn...  36.6 us
    ppermute x3, starting transfers between devices, per_device(): lax.ppermute(going_down, 'tp', [(d, (d - 1) % ways) for d in range(ways)])  10.8 us
    dot_general x5, matrix products, per_device(): jnp.einsum('sxcd,xdf->sxcf', arrived, going_up, preferred_element_type=jn...  10.5 us
    dot_general x1, matrix products, per_device(): jnp.einsum('sxcf,xdf->sxcd', hidden, down_piece, preferred_element_type=j...  8.55 us
    ppermute x2, starting transfers between devices, shifted(): return lax.ppermute(block, axis, route)  8.27 us
    unnamed x34, local copies, waits for them, and re-layouts  6.41 us
    dot_general x3, matrix products, per_device(): jnp.einsum('sxcd,xdf->sxcf', arrived, going_down, preferred_element_type=...  5.94 us
  transfers between devices with their start and end apart: 14, of which 6 were waited for; matrix products, arithmetic and copies ran while one was open for 23% of the time, Pallas kernels for 0%

profile of v1, /device:TPU:0, one launch (start us, length us, event | category | flops | bytes accessed | tf_op | source)
XLA Modules:
  0.0 207.2 jit_solution(10247556295352911677)
XLA Ops:
  8.8 1.2 constant_dynamic-slice_fusion
  10.1 4.9 %collective-permute-start.1 = (bf16[128,64]{0,1:T(8,128)(2,1)S(1)}, bf16[128,64]{0,1:T(8,128)(2,1)S(1)}, u32[]{:S(2)}, u32[]{:S(2)}) collective-permute-start(bf16[128,64]{0,1:T(8,128)(2,1)S(1)} %slice.36), channel_id=1, source_target_pairs={{0,8},{8,16},{16,24},{1,9},{9,17},{17,25},{2,10},{10,18},{18,26},{... | collective-permute-start | bytes 49160 | tf_op jit(solution)/shard_map/ppermute | solution.py:17
  15.2 3.4 %collective-permute-start = (bf16[128,64]{0,1:T(8,128)(2,1)S(1)}, bf16[128,64]{0,1:T(8,128)(2,1)S(1)}, u32[]{:S(2)}, u32[]{:S(2)}) collective-permute-start(bf16[128,64]{0,1:T(8,128)(2,1)S(1)} %slice.34), channel_id=1, source_target_pairs={{0,8},{8,16},{16,24},{1,9},{9,17},{17,25},{2,10},{10,18},{18,26},{... | collective-permute-start | bytes 49160 | tf_op jit(solution)/shard_map/ppermute | solution.py:17
  21.4 3.2 %convolution_convert_fusion = bf16[1024,2048]{1,0:T(8,128)(2,1)} fusion(bf16[128,2048]{1,0:T(8,128)(2,1)S(1)} %copy-done, bf16[16,8,8,128]{3,2,1,0:T(8,128)(2,1)S(1)} %bitcast.273), kind=kOutput, calls=%fused_computation.5 | convolution fusion | flops 538968064 | bytes 4980736 | tf_op jit(solution)/shard_map/dot_general | solution.py:86
  24.7 1.0 copy-done.2
  25.7 3.5 %collective-permute-start.6 = (bf16[1,2048,128]{2,1,0:T(8,128)(2,1)S(1)}, bf16[1,2048,128]{2,1,0:T(8,128)(2,1)}, u32[]{:S(2)}, u32[]{:S(2)}) collective-permute-start(bf16[1,2048,128]{2,1,0:T(8,128)(2,1)S(1)} %copy-done.2), channel_id=1, source_target_pairs={{0,7},{1,0},{2,1},{3,2},{4,3},{5,4},{6,5},{7,6},{8,15},{9,8},{10,9... | collective-permute-start | bytes 1572872 | tf_op jit(solution)/shard_map/ppermute | solution.py:136
  29.6 1.2 reduce-window.6
  31.7 20.8 %collective-permute-done.2 = bf16[1,2048,128]{2,1,0:T(8,128)(2,1)} collective-permute-done((bf16[1,2048,128]{2,1,0:T(8,128)(2,1)S(1)}, bf16[1,2048,128]{2,1,0:T(8,128)(2,1)}, u32[]{:S(2)}, u32[]{:S(2)}) %collective-permute-start.2) | collective-permute-done | bytes 524320 | tf_op jit(solution)/shard_map/ppermute | solution.py:135
  52.6 1.8 convolution_convert_fusion.1
  54.4 3.9 %all-to-all-start = ((bf16[4,1,96,2048]{3,2,1,0:T(8,128)(2,1)}), bf16[4,1,96,2048]{3,2,1,0:T(8,128)(2,1)S(1)}, u32[]{:S(2)}, u32[]{:S(2)}) async-start(bf16[4,1,96,2048]{3,2,1,0:T(8,128)(2,1)} %bitcast.272), calls=%async_computation.1 | async-start | bytes 3145728 | tf_op jit(solution)/shard_map/all_to_all | solution.py:119
  58.6 16.0 %collective-permute-done.3 = bf16[1,2048,128]{2,1,0:T(8,128)(2,1)} collective-permute-done((bf16[1,2048,128]{2,1,0:T(8,128)(2,1)}, bf16[1,2048,128]{2,1,0:T(8,128)(2,1)}, u32[]{:S(2)}, u32[]{:S(2)}) %collective-permute-start.3) | collective-permute-done | bytes 524320 | tf_op jit(solution)/shard_map/ppermute | solution.py:135
  75.0 3.6 %collective-permute-start.7 = (bf16[1,2048,128]{2,1,0:T(8,128)(2,1)}, bf16[1,2048,128]{2,1,0:T(8,128)(2,1)S(1)}, u32[]{:S(2)}, u32[]{:S(2)}) collective-permute-start(bf16[1,2048,128]{2,1,0:T(8,128)(2,1)} %collective-permute-done.6), channel_id=1, source_target_pairs={{0,7},{1,0},{2,1},{3,2},{4,3},{5,4},{6,5},{7,6},{8,15},{9,8},{10,9... | collective-permute-start | bytes 1572872 | tf_op jit(solution)/shard_map/ppermute | solution.py:136
  78.6 11.7 %collective-permute-done.4 = bf16[1,2048,128]{2,1,0:T(8,128)(2,1)} collective-permute-done((bf16[1,2048,128]{2,1,0:T(8,128)(2,1)}, bf16[1,2048,128]{2,1,0:T(8,128)(2,1)}, u32[]{:S(2)}, u32[]{:S(2)}) %collective-permute-start.4) | collective-permute-done | bytes 524320 | tf_op jit(solution)/shard_map/ppermute | solution.py:135
  90.7 2.3 %collective-permute-done.7 = bf16[1,2048,128]{2,1,0:T(8,128)(2,1)S(1)} collective-permute-done((bf16[1,2048,128]{2,1,0:T(8,128)(2,1)}, bf16[1,2048,128]{2,1,0:T(8,128)(2,1)S(1)}, u32[]{:S(2)}, u32[]{:S(2)}) %collective-permute-start.7) | collective-permute-done | bytes 524320 | tf_op jit(solution)/shard_map/ppermute | solution.py:136
  93.0 3.7 %collective-permute-start.8 = (bf16[1,2048,128]{2,1,0:T(8,128)(2,1)S(1)}, bf16[1,2048,128]{2,1,0:T(8,128)(2,1)}, u32[]{:S(2)}, u32[]{:S(2)}) collective-permute-start(bf16[1,2048,128]{2,1,0:T(8,128)(2,1)S(1)} %collective-permute-done.7), channel_id=1, source_target_pairs={{0,7},{1,0},{2,1},{3,2},{4,3},{5,4},{6,5},{7,6},{8,15},{9,8},{10,9... | collective-permute-start | bytes 1572872 | tf_op jit(solution)/shard_map/ppermute | solution.py:136
  96.6 20.6 %collective-permute-done.5 = bf16[1,2048,128]{2,1,0:T(8,128)(2,1)} collective-permute-done((bf16[1,2048,128]{2,1,0:T(8,128)(2,1)}, bf16[1,2048,128]{2,1,0:T(8,128)(2,1)}, u32[]{:S(2)}, u32[]{:S(2)}) %collective-permute-start.5) | collective-permute-done | bytes 524320 | tf_op jit(solution)/shard_map/ppermute | solution.py:135
  117.2 2.3 %constant_dynamic-update-slice_fusion.15 = (f32[4,1,96,2048]{3,2,0,1:T(8,128)}, f32[4,1,96,128]{3,2,0,1:T(8,128)S(1)}) fusion(bf16[1,2048,128]{2,1,0:T(8,128)(2,1)} %collective-permute-done.5, bf16[4,1,96,2048]{3,2,1,0:T(8,128)(2,1)S(1)} %all-to-all-done), kind=kOutput, calls=%fused_computation.110 | convolution fusion | flops 201326592 | bytes 2490368 | tf_op jit(solution)/shard_map/sxcd,xdf->sxcf/dot_general | solution.py:127
  119.6 2.3 %constant_dynamic-update-slice_fusion.14 = (f32[4,1,96,2048]{3,2,0,1:T(8,128)}, f32[4,1,96,128]{3,2,0,1:T(8,128)S(1)}) fusion(f32[4,1,96,2048]{3,2,0,1:T(8,128)} %get-tuple-element.8, bf16[1,2048,128]{2,1,0:T(8,128)(2,1)} %collective-permute-done.4, bf16[4,1,96,2048]{3,2,1,0:T(8,128)(2,1)S(1)} %all-to-all-done), kind=kOutput, calls=%fused_computation.109 | convolution fusion | flops 201326592 | bytes 2490368 | tf_op jit(solution)/shard_map/sxcd,xdf->sxcf/dot_general | solution.py:127
  121.9 2.3 %constant_dynamic-update-slice_fusion.13 = (f32[4,1,96,2048]{3,2,0,1:T(8,128)}, f32[4,1,96,128]{3,2,0,1:T(8,128)S(1)}) fusion(f32[4,1,96,2048]{3,2,0,1:T(8,128)} %get-tuple-element.10, bf16[1,2048,128]{2,1,0:T(8,128)(2,1)} %collective-permute-done.3, bf16[4,1,96,2048]{3,2,1,0:T(8,128)(2,1)S(1)} %all-to-all-done), kind=kOutput, calls=%fused_computation.108 | convolution fusion | flops 201326592 | bytes 2490368 | tf_op jit(solution)/shard_map/sxcd,xdf->sxcf/dot_general | solution.py:127
  124.2 2.3 %constant_dynamic-update-slice_fusion.12 = (f32[4,1,96,2048]{3,2,0,1:T(8,128)}, f32[4,1,96,128]{3,2,0,1:T(8,128)S(1)}) fusion(f32[4,1,96,2048]{3,2,0,1:T(8,128)} %get-tuple-element.12, bf16[1,2048,128]{2,1,0:T(8,128)(2,1)} %collective-permute-done.2, bf16[4,1,96,2048]{3,2,1,0:T(8,128)(2,1)S(1)} %all-to-all-done), kind=kOutput, calls=%fused_computation.107 | convolution fusion | flops 201326592 | bytes 2490368 | tf_op jit(solution)/shard_map/sxcd,xdf->sxcf/dot_general | solution.py:127
  126.5 1.3 constant_dynamic-update-slice_fusion.11
  127.8 2.3 %constant_dynamic-update-slice_fusion.10 = (f32[4,1,96,2048]{3,2,0,1:T(8,128)}, f32[4,1,96,128]{3,2,0,1:T(8,128)S(1)}) fusion(f32[4,1,96,2048]{3,2,0,1:T(8,128)} %get-tuple-element.16, bf16[1,2048,128]{2,1,0:T(8,128)(2,1)} %collective-permute-done.6, bf16[4,1,96,2048]{3,2,1,0:T(8,128)(2,1)S(1)} %all-to-all-done), kind=kOutput, calls=%fused_computation.105 | convolution fusion | flops 201326592 | bytes 2490368 | tf_op jit(solution)/shard_map/sxcd,xdf->sxcf/dot_general | solution.py:131
  130.1 1.3 constant_dynamic-update-slice_fusion.9
  131.4 2.4 %constant_dynamic-update-slice_fusion.8 = (f32[4,1,96,2048]{3,2,0,1:T(8,128)}, f32[4,1,96,128]{3,2,0,1:T(8,128)S(1)}) fusion(f32[4,1,96,2048]{3,2,0,1:T(8,128)} %get-tuple-element.20, bf16[1,2048,128]{2,1,0:T(8,128)(2,1)} %collective-permute-done.8, bf16[4,1,96,2048]{3,2,1,0:T(8,128)(2,1)S(1)} %all-to-all-done), kind=kOutput, calls=%fused_computation.103 | convolution fusion | flops 201326592 | bytes 2490368 | tf_op jit(solution)/shard_map/sxcd,xdf->sxcf/dot_general | solution.py:131
  139.4 8.6 %fusion.7 = bf16[4,1,96,2048]{3,2,1,0:T(8,128)(2,1)} fusion(bf16[1,2048,1024]{2,1,0:T(8,128)(2,1)} %all-gather.5.cloned.1.call-done, bf16[1,2048,1024]{2,1,0:T(8,128)(2,1)} %all-gather.3.cloned.1.call-done, bf16[4,1,96,2048]{3,2,1,0:T(8,128)(2,1)S(1)} %all-to-all-done, f32[4,1,96,2048]{3,2,0,1:T(8,128)} %constant_dynamic-update-slice_fusion, s32[]{:T(128)S(6)} %select_n.64), kind=kOutput, calls=%fused_computation.8 | convolution fusion | flops 3224371200 | bytes 13107204 | tf_op jit(solution)/shard_map/sxcf,xdf->sxcd/dot_general | solution.py:141
  148.0 5.4 %all-to-all-start.1 = ((bf16[4,1,96,2048]{3,2,1,0:T(8,128)(2,1)}), bf16[4,1,96,2048]{3,2,1,0:T(8,128)(2,1)S(1)}, u32[]{:S(2)}, u32[]{:S(2)}) async-start(bf16[4,1,96,2048]{3,2,1,0:T(8,128)(2,1)} %fusion.7), calls=%async_computation.2 | async-start | bytes 3145728 | tf_op jit(solution)/shard_map/all_to_all | solution.py:142
  153.5 36.6 %reduce-scatter.2.cloned.1.call-done = bf16[128,2048]{1,0:T(8,128)(2,1)} async-done(((bf16[1024,2048]{1,0:T(8,128)(2,1)}), bf16[128,2048]{1,0:T(8,128)(2,1)}) %reduce-scatter.2.cloned.1.call-update) | async-done | bytes 524304 | tf_op jit(solution)/shard_map/reduce_scatter | solution.py:85
  190.1 1.2 fusion.64
  191.3 2.0 fusion.66
  193.4 1.4 gather_fusion
  195.5 4.1 %multiply_reduce_fusion = f32[128,2048]{1,0:T(8,128)S(1)} fusion(bf16[128,2,2048]{2,1,0:T(2,128)(2,1)S(1)} %gather.7, pred[128,2]{1,0:T(8,128)(4,1)S(1)} %copy.102, f32[128,2]{1,0:T(8,128)S(1)} %copy.96), kind=kLoop, calls=%fused_computation.11 | loop fusion | flops 1835008 | bytes 2098432 | tf_op jit(solution)/shard_map/reduce_sum | solution.py:149
  199.7 1.0 multiply_convert_fusion
  (107 shorter events, 13.6 us)
Async XLA Ops:
  7.2 14.3 %copy-start = (bf16[128,2048]{1,0:T(8,128)(2,1)S(1)}, bf16[128,2048]{1,0:T(8,128)(2,1)}, u32[]{:S(2)}) copy-start(bf16[128,2048]{1,0:T(8,128)(2,1)} %param.21) | copy-start | bytes 1572868
  7.2 12.0 %copy-start.9 = (f32[2]{0:T(128)S(1)}, f32[2]{0:T(128)}, u32[]{:S(2)}) copy-start(f32[2]{0:T(128)} %param.19) | copy-start | bytes 28
  7.2 132.2 %all-gather.3.cloned.1.call-start = ((), (), s32[]{:S(2)}) async-start(), calls=%async_computation.4 | async-start | bytes 4718592 | tf_op jit(solution)/shard_map/all_gather | solution.py:120
  7.9 11.4 %copy-start.3 = (bf16[1024,128]{1,0:T(8,128)(2,1)S(1)}, bf16[1024,128]{1,0:T(8,128)(2,1)}, u32[]{:S(2)}) copy-start(bf16[1024,128]{1,0:T(8,128)(2,1)} %param.16) | copy-start | bytes 786436
  7.9 131.5 %all-gather.5.cloned.1.call-start = ((), (), s32[]{:S(2)}) async-start(), calls=%async_computation.5 | async-start | bytes 4718592 | tf_op jit(solution)/shard_map/all_gather | solution.py:121
  8.7 181.4 %reduce-scatter.2.cloned.1.call-start = ((), (), s32[]{:S(2)}) async-start(), calls=%async_computation.3 | async-start | bytes 4718592 | tf_op jit(solution)/shard_map/reduce_scatter | solution.py:85
  10.1 9.4 %collective-permute-start.1 = (bf16[128,64]{0,1:T(8,128)(2,1)S(1)}, bf16[128,64]{0,1:T(8,128)(2,1)S(1)}, u32[]{:S(2)}, u32[]{:S(2)}) collective-permute-start(bf16[128,64]{0,1:T(8,128)(2,1)S(1)} %slice.36), channel_id=1, source_target_pairs={{0,8},{8,16},{16,24},{1,9},{9,17},{17,25},{2,10},{10,18},{18,26},{... | collective-permute-start | bytes 49160 | tf_op jit(solution)/shard_map/ppermute | solution.py:17
  15.2 5.6 %collective-permute-start = (bf16[128,64]{0,1:T(8,128)(2,1)S(1)}, bf16[128,64]{0,1:T(8,128)(2,1)S(1)}, u32[]{:S(2)}, u32[]{:S(2)}) collective-permute-start(bf16[128,64]{0,1:T(8,128)(2,1)S(1)} %slice.34), channel_id=1, source_target_pairs={{0,8},{8,16},{16,24},{1,9},{9,17},{17,25},{2,10},{10,18},{18,26},{... | collective-permute-start | bytes 49160 | tf_op jit(solution)/shard_map/ppermute | solution.py:17
  19.6 0.7 copy-start.8
  24.6 1.0 copy-start.2
  24.6 4.6 %copy-start.4 = (s32[128,2]{0,1:T(2,128)S(1)}, s32[128,2]{0,1:T(2,128)}, u32[]{:S(2)}) copy-start(s32[128,2]{0,1:T(2,128)} %param.28) | copy-start | bytes 3076
  24.6 6.8 %copy-start.1 = (bf16[128,2048]{1,0:T(8,128)(2,1)S(1)}, bf16[128,2048]{1,0:T(8,128)(2,1)}, u32[]{:S(2)}) copy-start(bf16[128,2048]{1,0:T(8,128)(2,1)} %param.23) | copy-start | bytes 1572868
  24.7 27.9 %copy-start.5 = (f32[2048]{0:T(1024)S(1)}, f32[2048]{0:T(1024)}, u32[]{:S(2)}) copy-start(f32[2048]{0:T(1024)} %param.24) | copy-start | bytes 24580
  25.7 26.8 %collective-permute-start.2 = (bf16[1,2048,128]{2,1,0:T(8,128)(2,1)S(1)}, bf16[1,2048,128]{2,1,0:T(8,128)(2,1)}, u32[]{:S(2)}, u32[]{:S(2)}) collective-permute-start(bf16[1,2048,128]{2,1,0:T(8,128)(2,1)S(1)} %copy-done.2), channel_id=1, source_target_pairs={{0,1},{1,2},{2,3},{3,4},{4,5},{5,6},{6,7},{7,0},{8,9},{9,10},{10,1... | collective-permute-start | bytes 1572872 | tf_op jit(solution)/shard_map/ppermute | solution.py:135
  25.7 49.3 %collective-permute-start.6 = (bf16[1,2048,128]{2,1,0:T(8,128)(2,1)S(1)}, bf16[1,2048,128]{2,1,0:T(8,128)(2,1)}, u32[]{:S(2)}, u32[]{:S(2)}) collective-permute-start(bf16[1,2048,128]{2,1,0:T(8,128)(2,1)S(1)} %copy-done.2), channel_id=1, source_target_pairs={{0,7},{1,0},{2,1},{3,2},{4,3},{5,4},{6,5},{7,6},{8,15},{9,8},{10,9... | collective-permute-start | bytes 1572872 | tf_op jit(solution)/shard_map/ppermute | solution.py:136
  52.5 22.1 %collective-permute-start.3 = (bf16[1,2048,128]{2,1,0:T(8,128)(2,1)}, bf16[1,2048,128]{2,1,0:T(8,128)(2,1)}, u32[]{:S(2)}, u32[]{:S(2)}) collective-permute-start(bf16[1,2048,128]{2,1,0:T(8,128)(2,1)} %collective-permute-done.2), channel_id=1, source_target_pairs={{0,1},{1,2},{2,3},{3,4},{4,5},{5,6},{6,7},{7,0},{8,9},{9,10},{10,1... | collective-permute-start | bytes 1572872 | tf_op jit(solution)/shard_map/ppermute | solution.py:135
  54.4 3.9 %copy-start.10 = (bf16[2048,4]{0,1:T(4,128)(2,1)S(1)}, bf16[2048,4]{0,1:T(4,128)(2,1)}, u32[]{:S(2)}) copy-start(bf16[2048,4]{0,1:T(4,128)(2,1)} %param.26) | copy-start | bytes 49156
  54.4 20.3 %copy-start.11 = (bf16[2048,4]{0,1:T(4,128)(2,1)S(1)}, bf16[2048,4]{0,1:T(4,128)(2,1)}, u32[]{:S(2)}) copy-start(bf16[2048,4]{0,1:T(4,128)(2,1)} %param.27) | copy-start | bytes 49156
  54.4 42.2 %all-to-all-start = ((bf16[4,1,96,2048]{3,2,1,0:T(8,128)(2,1)}), bf16[4,1,96,2048]{3,2,1,0:T(8,128)(2,1)S(1)}, u32[]{:S(2)}, u32[]{:S(2)}) async-start(bf16[4,1,96,2048]{3,2,1,0:T(8,128)(2,1)} %bitcast.272), calls=%async_computation.1 | async-start | bytes 3145728 | tf_op jit(solution)/shard_map/all_to_all | solution.py:119
  74.6 15.6 %collective-permute-start.4 = (bf16[1,2048,128]{2,1,0:T(8,128)(2,1)}, bf16[1,2048,128]{2,1,0:T(8,128)(2,1)}, u32[]{:S(2)}, u32[]{:S(2)}) collective-permute-start(bf16[1,2048,128]{2,1,0:T(8,128)(2,1)} %collective-permute-done.3), channel_id=1, source_target_pairs={{0,1},{1,2},{2,3},{3,4},{4,5},{5,6},{6,7},{7,0},{8,9},{9,10},{10,1... | collective-permute-start | bytes 1572872 | tf_op jit(solution)/shard_map/ppermute | solution.py:135
  75.0 18.0 %collective-permute-start.7 = (bf16[1,2048,128]{2,1,0:T(8,128)(2,1)}, bf16[1,2048,128]{2,1,0:T(8,128)(2,1)S(1)}, u32[]{:S(2)}, u32[]{:S(2)}) collective-permute-start(bf16[1,2048,128]{2,1,0:T(8,128)(2,1)} %collective-permute-done.6), channel_id=1, source_target_pairs={{0,7},{1,0},{2,1},{3,2},{4,3},{5,4},{6,5},{7,6},{8,15},{9,8},{10,9... | collective-permute-start | bytes 1572872 | tf_op jit(solution)/shard_map/ppermute | solution.py:136
  90.2 27.0 %collective-permute-start.5 = (bf16[1,2048,128]{2,1,0:T(8,128)(2,1)}, bf16[1,2048,128]{2,1,0:T(8,128)(2,1)}, u32[]{:S(2)}, u32[]{:S(2)}) collective-permute-start(bf16[1,2048,128]{2,1,0:T(8,128)(2,1)} %collective-permute-done.4), channel_id=1, source_target_pairs={{0,1},{1,2},{2,3},{3,4},{4,5},{5,6},{6,7},{7,0},{8,9},{9,10},{10,1... | collective-permute-start | bytes 1572872 | tf_op jit(solution)/shard_map/ppermute | solution.py:135
  93.0 38.4 %collective-permute-start.8 = (bf16[1,2048,128]{2,1,0:T(8,128)(2,1)S(1)}, bf16[1,2048,128]{2,1,0:T(8,128)(2,1)}, u32[]{:S(2)}, u32[]{:S(2)}) collective-permute-start(bf16[1,2048,128]{2,1,0:T(8,128)(2,1)S(1)} %collective-permute-done.7), channel_id=1, source_target_pairs={{0,7},{1,0},{2,1},{3,2},{4,3},{5,4},{6,5},{7,6},{8,15},{9,8},{10,9... | collective-permute-start | bytes 1572872 | tf_op jit(solution)/shard_map/ppermute | solution.py:136
  148.0 43.4 %copy-start.6 = (f32[2048]{0:T(1024)S(1)}, f32[2048]{0:T(1024)}, u32[]{:S(2)}) copy-start(f32[2048]{0:T(1024)} %param.22) | copy-start | bytes 24580
  148.0 45.4 %all-to-all-start.1 = ((bf16[4,1,96,2048]{3,2,1,0:T(8,128)(2,1)}), bf16[4,1,96,2048]{3,2,1,0:T(8,128)(2,1)S(1)}, u32[]{:S(2)}, u32[]{:S(2)}) async-start(bf16[4,1,96,2048]{3,2,1,0:T(8,128)(2,1)} %fusion.7), calls=%async_computation.2 | async-start | bytes 3145728 | tf_op jit(solution)/shard_map/all_to_all | solution.py:142
  195.5 4.3 %copy-start.7 = (f32[2048]{0:T(1024)S(1)}, f32[2048]{0:T(1024)}, u32[]{:S(2)}) copy-start(f32[2048]{0:T(1024)} %param.25) | copy-start | bytes 24580
Sparse Core Ops, SparseCore 0:
  9.6 67.3 all-gather.2
  78.6 59.6 all-gather.4
  140.6 49.4 reduce-scatter.1
